TPU v7x, 512 devices: a whole 4x4x16 slice. The times are simulated.
512 devices in a mesh: fs: 16 (over y, x), tp: 32 (over z, core).
Axes of the slice: x: 4, y: 4, z: 16, core: 2. Of those that a mesh axis runs over, the one named last changes fastest.
Arguments:
- saved_input: bfloat16 [16384, 4096], P('fs', 'tp'), may hold values from -6 to 6
- query_cot: bfloat16 [16384, 4096], P('fs', 'tp'), may hold values from -6 to 6
- key_cot: bfloat16 [16384, 4096], P('fs', 'tp'), may hold values from -6 to 6
- query_master: float32 [4096, 4096], P('fs', 'tp'), may hold values from -0.09375 to 0.09375
- key_master: float32 [4096, 4096], P('fs', 'tp'), may hold values from -0.09375 to 0.09375
- query_basis: bfloat16 [4096, 256], P('fs'), may hold values from -3 to 3
- key_basis: bfloat16 [4096, 256], P('fs'), may hold values from -3 to 3
- query_first: float32 [256, 4096], P('fs', 'tp'), may hold values from -240 to 240
- query_second: float32 [256, 4096], P('fs', 'tp'), may hold values from 1000 to 20000
- key_first: float32 [256, 4096], P('fs', 'tp'), may hold values from -240 to 240
- key_second: float32 [256, 4096], P('fs', 'tp'), may hold values from 1000 to 20000
Outputs:
- query_step: float32 [4096, 4096], P('fs', 'tp')
- query_weight: float32 [4096, 4096], P('fs', 'tp')
- query_copy: bfloat16 [4096, 4096], P(None, 'tp')
- query_first_new: float32 [256, 4096], P('fs', 'tp')
- query_second_new: float32 [256, 4096], P('fs', 'tp')
- key_step: float32 [4096, 4096], P('fs', 'tp')
- key_weight: float32 [4096, 4096], P('fs', 'tp')
- key_copy: bfloat16 [4096, 4096], P(None, 'tp')
- key_first_new: float32 [256, 4096], P('fs', 'tp')
- key_second_new: float32 [256, 4096], P('fs', 'tp')
All inputs are finite; a program needn't handle non-finite values.
Results may differ from a plain program's by a relative error of at most 0.0065.
Values may be sent and summed in bfloat16 or wider, within the bound.
A program may use at most 64 MiB of HBM per device.

v0:
```python
import jax
import jax.numpy as jnp
from jax import lax
from jax.sharding import Mesh
from jax.sharding import PartitionSpec as P

D = 4096
HD = 128
FS = ("fs_0", "fs_1")
moment_decay = 0.8
square_decay = 0.9
square_floor = 1.0
norm_floor = 0.01
step_rate = 0.01


def in_one_piece(arrays, axis, dim, along):
    widths = [a.shape[along] for a in arrays]
    both = jnp.concatenate(arrays, axis=along)
    out = lax.all_gather(both, axis, axis=dim, tiled=True)
    return tuple(jnp.split(out, [sum(widths[:k]) for k in range(1, len(widths))], axis=along))


def cut_along(x, dim, count):
    lengths = x.shape
    pieces = x.reshape(*lengths[:dim], count, lengths[dim] // count, *lengths[dim + 1 :])
    return jnp.moveaxis(pieces, dim, 0)


def sent_and_summed(x, axis, dim):
    count = lax.axis_size(axis)
    pieces = lax.all_to_all(cut_along(x, dim, count), axis, 0, 0, tiled=True)
    return jnp.sum(pieces, axis=0)


def sent_to_all(x, axis):
    count = lax.axis_size(axis)
    return lax.all_to_all(jnp.broadcast_to(x[None], (count, *x.shape)), axis, 0, 0, tiled=True)


def in_order(pieces, dim):
    lengths = list(pieces.shape[1:])
    lengths[dim] *= pieces.shape[0]
    return jnp.moveaxis(pieces, 0, dim).reshape(lengths)


def gathered_copies(x, axis, dim):
    pieces = sent_to_all(x, axis)
    return in_order(pieces, dim)


def by_axis(x, axes):
    for axis in axes:
        x = lax.psum(x, axis)
    return x


def split_product(low_part, cot_part):
    upper = low_part.astype(jnp.bfloat16)
    lower = (low_part - upper.astype(jnp.float32)).astype(jnp.bfloat16)
    return jnp.dot(upper.T, cot_part, preferred_element_type=jnp.float32) + jnp.dot(
        lower.T, cot_part, preferred_element_type=jnp.float32
    )


def cot_rows(query_low, key_low, cot_wide, width):

    def low_rows(start, count):
        return jnp.concatenate(
            [
                split_product(query_low, cot_wide[:, :width]),
                split_product(key_low, cot_wide[:, width:]),
            ],
            axis=1,
        )

    return low_rows


def head_squares(update):
    by_head = update.reshape(update.shape[0], -1, HD)
    return jnp.sum(by_head * by_head, axis=(0, 2))


def apply_scale(update, total):
    scale = 1.0 / jnp.sqrt(total / (D * HD) + norm_floor)
    by_head = update.reshape(update.shape[0], -1, HD)
    return (by_head * scale[None, :, None]).reshape(update.shape)


def body(
    saved_input,
    query_cot,
    key_cot,
    query_master,
    key_master,
    query_basis,
    key_basis,
    query_first,
    query_second,
    key_first,
    key_second,
):
    width = query_cot.shape[1]
    low_count = query_first.shape[0]
    cotangents = jnp.concatenate([query_cot, key_cot], axis=1)
    inputs = lax.all_gather(saved_input, "tp", axis=1, tiled=True)
    bases = in_one_piece((query_basis, key_basis), FS, 0, 1)
    query_low = jnp.dot(inputs, bases[0], preferred_element_type=jnp.float32)
    key_low = jnp.dot(inputs, bases[1], preferred_element_type=jnp.float32)
    low_rows = cot_rows(query_low, key_low, cotangents, width)
    projected = sent_and_summed(low_rows(jnp.int32(0), low_count * lax.axis_size(FS)), FS, 0)
    firsts = jnp.concatenate([query_first, key_first], axis=1)
    seconds = jnp.concatenate([query_second, key_second], axis=1)
    first_new = moment_decay * firsts + (1.0 - moment_decay) * projected
    second_new = square_decay * seconds + (1.0 - square_decay) * projected * projected
    ratio = (first_new / jnp.sqrt(second_new + square_floor)).astype(jnp.bfloat16)
    piece = gathered_copies(ratio, FS, 0)
    query_update = jnp.dot(query_basis, piece[:, :width], preferred_element_type=jnp.float32)
    key_update = jnp.dot(key_basis, piece[:, width:], preferred_element_type=jnp.float32)
    query_total, key_total = (
        by_axis(head_squares(query_update), FS),
        by_axis(head_squares(key_update), FS),
    )
    query_step = apply_scale(query_update, query_total)
    key_step = apply_scale(key_update, key_total)
    query_weight = query_master - step_rate * query_step
    key_weight = key_master - step_rate * key_step
    copies = in_one_piece(
        (query_weight.astype(jnp.bfloat16), key_weight.astype(jnp.bfloat16)), FS, 0, 1
    )
    return (
        query_step,
        query_weight,
        copies[0],
        first_new[:, :width],
        second_new[:, :width],
        key_step,
        key_weight,
        copies[1],
        first_new[:, width:],
        second_new[:, width:],
    )


def solution(mesh):
    torus = Mesh(mesh.devices.reshape(4, 4, mesh.shape["tp"]), ("fs_0", "fs_1", "tp"))
    in_specs = (
        P(FS, "tp"),
        P(FS, "tp"),
        P(FS, "tp"),
        P(FS, "tp"),
        P(FS, "tp"),
        P(FS, None),
        P(FS, None),
        P(FS, "tp"),
        P(FS, "tp"),
        P(FS, "tp"),
        P(FS, "tp"),
    )
    out_specs = (
        P(FS, "tp"),
        P(FS, "tp"),
        P(None, "tp"),
        P(FS, "tp"),
        P(FS, "tp"),
        P(FS, "tp"),
        P(FS, "tp"),
        P(None, "tp"),
        P(FS, "tp"),
        P(FS, "tp"),
    )
    return jax.shard_map(body, mesh=torus, in_specs=in_specs, out_specs=out_specs, check_vma=False)
```

profile of v0, /device:TPU:2, one launch (start us, length us, event | category | flops | bytes accessed | tf_op | source)
XLA Modules:
  0.0 306.8 jit_solution(4869370095504522026)
XLA Ops:
  7.2 1.7 pad_maximum_fusion
  9.0 0.7 all-gather.6.cloned.1.call-update
  9.7 73.1 %all-gather.4.cloned.1.call-done = bf16[4096,512]{1,0:T(8,128)(2,1)} async-done(((bf16[256,512]{1,0:T(8,128)(2,1)}), bf16[4096,512]{1,0:T(8,128)(2,1)}) %all-gather.4.cloned.1.call-update) | async-done | bytes 4194320 | tf_op jit(solution)/shard_map/all_gather | solution.py:20
  82.8 97.5 %all-gather.6.cloned.1.call-done = bf16[1024,4096]{1,0:T(8,128)(2,1)} async-done(((bf16[1024,128]{1,0:T(8,128)(2,1)}), bf16[1024,4096]{1,0:T(8,128)(2,1)}) %all-gather.6.cloned.1.call-update) | async-done | bytes 8388624 | tf_op jit(solution)/shard_map/all_gather | solution.py:107
  180.2 6.5 %fusion.4 = f32[1024,256]{0,1:T(8,128)S(1)} fusion(bf16[1024,4096]{1,0:T(8,128)(2,1)} %all-gather.6.cloned.1.call-done, bf16[4096,512]{1,0:T(8,128)(2,1)} %all-gather.4.cloned.1.call-done), kind=kOutput, calls=%fused_computation.4 | convolution fusion | flops 2147483648 | bytes 11534336 | tf_op jit(solution)/shard_map/dot_general | solution.py:109
  186.8 0.3 fusion.14
  187.1 0.3 convolution_add_fusion.1
  187.5 0.4 copy-done.11
  187.8 2.4 fusion.7
  190.3 0.3 fusion.11
  190.7 0.3 convolution_add_fusion
  191.0 0.1 copy.29
  191.1 14.8 %all_to_all.10 = f32[16,16,256]{2,1,0:T(8,128)S(1)} all-to-all(f32[16,16,256]{2,1,0:T(8,128)S(1)} %bitcast.24), channel_id=1, replica_groups=mesh['fs_0'=4,'fs_1'=4,'tp'=32] {'fs_0','fs_1'}, dimensions={0} | all-to-all | bytes 524288 | tf_op jit(solution)/shard_map/all_to_all | solution.py:32
  206.0 0.7 broadcast_in_dim.2
  206.7 4.8 %all-to-all-start.1 = ((bf16[16,16,256]{2,1,0:T(8,128)(2,1)}), bf16[16,16,256]{2,1,0:T(8,128)(2,1)S(1)}, u32[]{:S(2)}, u32[]{:S(2)}) async-start(bf16[16,16,256]{2,1,0:T(8,128)(2,1)} %broadcast_in_dim.2), calls=%async_computation.1 | async-start | bytes 262144 | tf_op jit(solution)/shard_map/all_to_all | solution.py:38
  211.5 0.1 copy.30
  211.6 0.1 copy.31
  211.7 6.4 %all-to-all-done.1 = bf16[16,16,256]{2,1,0:T(8,128)(2,1)S(1)} async-done(((bf16[16,16,256]{2,1,0:T(8,128)(2,1)}), bf16[16,16,256]{2,1,0:T(8,128)(2,1)S(1)}, u32[]{:S(2)}, u32[]{:S(2)}) %all-to-all-start.1) | async-done | bytes 131104 | tf_op jit(solution)/shard_map/all_to_all | solution.py:38
  218.2 0.8 multiply_reduce_fusion.1
  219.0 0.8 multiply_reduce_fusion
  219.8 9.2 %all-reduce.1 = (f32[1]{0:T(128)}, f32[1]{0:T(128)}) all-reduce(f32[1]{0:T(128)} %bitcast.4, f32[1]{0:T(128)} %bitcast.7), channel_id=1, replica_groups=mesh['fs_0'=4,'fs_1'=4,'tp'=32] {'fs_0'}, use_global_device_ids=true, to_apply=%region_2.0 | all-reduce | flops 2 | bytes 16 | tf_op jit(solution)/shard_map/psum | solution.py:54
  229.0 9.8 %all-reduce = (f32[1]{0:T(128)}, f32[1]{0:T(128)}) all-reduce(f32[1]{0:T(128)} %get-tuple-element.32, f32[1]{0:T(128)} %get-tuple-element.33), channel_id=1, replica_groups=mesh['fs_0'=4,'fs_1'=4,'tp'=32] {'fs_1'}, use_global_device_ids=true, to_apply=%region_3.0 | all-reduce | flops 2 | bytes 16 | tf_op jit(solution)/shard_map/psum | solution.py:54
  240.2 0.7 pad_maximum_fusion.2
  240.9 0.6 fusion.27
  241.5 0.8 copy.32
  242.3 0.8 copy.33
  243.1 0.8 copy.35
  243.8 0.8 copy.36
  244.6 51.4 %all-gather.8.cloned.1.call-done = bf16[4096,256]{0,1:T(8,128)(2,1)} async-done(((bf16[256,256]{0,1:T(8,128)(2,1)}), bf16[4096,256]{0,1:T(8,128)(2,1)}) %all-gather.8.cloned.1.call-update) | async-done | bytes 2097168 | tf_op jit(solution)/shard_map/all_gather | solution.py:20
  296.0 1.7 fusion.26
  297.6 1.3 copy.34
  299.0 1.3 copy.37
  (32 shorter events, 0.3 us)
Async XLA Ops:
  7.2 179.6 %copy-start = (bf16[1024,128]{1,0:T(8,128)(2,1)S(1)}, bf16[1024,128]{1,0:T(8,128)(2,1)}, u32[]{:S(2)}) copy-start(bf16[1024,128]{1,0:T(8,128)(2,1)} %param.12) | copy-start | bytes 786436
  7.2 75.6 %all-gather.4.cloned.1.call-start = ((), (), s32[]{:S(2)}) async-start(), calls=%async_computation.2 | async-start | bytes 4456448 | tf_op jit(solution)/shard_map/all_gather | solution.py:20
  9.0 171.3 %all-gather.6.cloned.1.call-start = ((), (), s32[]{:S(2)}) async-start(), calls=%async_computation.3 | async-start | bytes 8650752 | tf_op jit(solution)/shard_map/all_gather | solution.py:107
  180.2 7.2 %copy-start.10 = (bf16[1024,4096]{1,0:T(8,128)(2,1)S(1)}, bf16[1024,4096]{1,0:T(8,128)(2,1)}, u32[]{:S(2)}) copy-start(bf16[1024,4096]{1,0:T(8,128)(2,1)} %all-gather.6.cloned.1.call-done) | copy-start | bytes 25165828
  180.2 7.6 %copy-start.11 = (bf16[4096,512]{1,0:T(8,128)(2,1)S(1)}, bf16[4096,512]{1,0:T(8,128)(2,1)}, u32[]{:S(2)}) copy-start(bf16[4096,512]{1,0:T(8,128)(2,1)} %all-gather.4.cloned.1.call-done) | copy-start | bytes 12582916
  187.8 2.4 copy-start.1
  190.2 15.7 %copy-start.6 = (f32[16,128]{1,0:T(8,128)S(1)}, f32[16,128]{1,0:T(8,128)}, u32[]{:S(2)}) copy-start(f32[16,128]{1,0:T(8,128)} %param.21) | copy-start | bytes 24580
  190.2 15.7 %copy-start.7 = (f32[16,128]{1,0:T(8,128)S(1)}, f32[16,128]{1,0:T(8,128)}, u32[]{:S(2)}) copy-start(f32[16,128]{1,0:T(8,128)} %param.19) | copy-start | bytes 24580
  190.3 15.7 %copy-start.8 = (f32[16,128]{1,0:T(8,128)S(1)}, f32[16,128]{1,0:T(8,128)}, u32[]{:S(2)}) copy-start(f32[16,128]{1,0:T(8,128)} %param.20) | copy-start | bytes 24580
  190.3 15.7 %copy-start.9 = (f32[16,128]{1,0:T(8,128)S(1)}, f32[16,128]{1,0:T(8,128)}, u32[]{:S(2)}) copy-start(f32[16,128]{1,0:T(8,128)} %param.18) | copy-start | bytes 24580
  190.3 21.2 %copy-start.4 = (f32[256,128]{1,0:T(8,128)S(1)}, f32[256,128]{1,0:T(8,128)}, u32[]{:S(2)}) copy-start(f32[256,128]{1,0:T(8,128)} %param.14) | copy-start | bytes 393220
  190.3 21.3 %copy-start.5 = (f32[256,128]{1,0:T(8,128)S(1)}, f32[256,128]{1,0:T(8,128)}, u32[]{:S(2)}) copy-start(f32[256,128]{1,0:T(8,128)} %param.15) | copy-start | bytes 393220
  190.3 27.9 %copy-start.2 = (bf16[256,256]{1,0:T(8,128)(2,1)S(1)}, bf16[256,256]{1,0:T(8,128)(2,1)}, u32[]{:S(2)}) copy-start(bf16[256,256]{1,0:T(8,128)(2,1)} %param.16) | copy-start | bytes 393220
  190.3 28.7 %copy-start.3 = (bf16[256,256]{1,0:T(8,128)(2,1)S(1)}, bf16[256,256]{1,0:T(8,128)(2,1)}, u32[]{:S(2)}) copy-start(bf16[256,256]{1,0:T(8,128)(2,1)} %param.17) | copy-start | bytes 393220
  206.7 11.5 %all-to-all-start.1 = ((bf16[16,16,256]{2,1,0:T(8,128)(2,1)}), bf16[16,16,256]{2,1,0:T(8,128)(2,1)S(1)}, u32[]{:S(2)}, u32[]{:S(2)}) async-start(bf16[16,16,256]{2,1,0:T(8,128)(2,1)} %broadcast_in_dim.2), calls=%async_computation.1 | async-start | bytes 262144 | tf_op jit(solution)/shard_map/all_to_all | solution.py:38
  211.5 84.5 %all-gather.8.cloned.1.call-start = ((), (), s32[]{:S(2)}) async-start(), calls=%async_computation.4 | async-start | bytes 2228224 | tf_op jit(solution)/shard_map/all_gather | solution.py:20
Sparse Core Ops, SparseCore 0:
  11.6 71.1 all-gather.3
  84.8 95.3 all-gather.5
  241.1 54.8 all-gather.7
where the time goes:
time: 307 us
  waiting for transfers between devices  229 us (75%)
  blocking collectives  33.8 us (11%)
  between operations  15.4 us (5%)
  matrix products  11.8 us (4%)
  local copies, waits for them, and re-layouts  9.34 us (3%)
  starting transfers between devices  4.88 us (2%)
    all_gather x2, waiting for transfers between devices, in_one_piece(): out = lax.all_gather(both, axis, axis=dim, tiled=True)  124 us
    all_gather x1, waiting for transfers between devices, body(): inputs = lax.all_gather(saved_input, 'tp', axis=1, tiled=True)  97.5 us
    psum x2, blocking collectives, by_axis(): x = lax.psum(x, axis)  19 us
    all_to_all x1, blocking collectives, sent_and_summed(): pieces = lax.all_to_all(cut_along(x, dim, count), axis, 0, 0, tiled=True)  14.8 us
    dot_general x1, matrix products, body(): query_low = jnp.dot(inputs, bases[0], preferred_element_type=jnp.float32)  6.54 us
    all_to_all x1, waiting for transfers between devices, sent_to_all(): lax.all_to_all(jnp.broadcast_to(x[None], (count, *x.shape)), axis, 0, 0,...  6.45 us
    unnamed x32, local copies, waits for them, and re-layouts  6.25 us
  transfers between devices with their start and end apart: 4, of which 4 were waited for; matrix products, arithmetic and copies ran while one was open for 1% of the time, Pallas kernels for 0%

commit v1 on v0

--- a/solution.py
+++ b/solution.py
@@ -104,7 +104,7 @@
     width = query_cot.shape[1]
     low_count = query_first.shape[0]
     cotangents = jnp.concatenate([query_cot, key_cot], axis=1)
-    inputs = lax.all_gather(saved_input, "tp", axis=1, tiled=True)
+    inputs = jnp.concatenate(lax.all_gather(saved_input, "tp"), axis=1)
     bases = in_one_piece((query_basis, key_basis), FS, 0, 1)
     query_low = jnp.dot(inputs, bases[0], preferred_element_type=jnp.float32)
     key_low = jnp.dot(inputs, bases[1], preferred_element_type=jnp.float32)

time: 307 us -> 291 us (0.948)
  waiting for transfers between devices: 229 us -> 203 us
  local copies, waits for them, and re-layouts: 9.34 us -> 20.8 us
    all_gather x1, waiting for transfers between devices: 97.5 us -> 83.7 us  [body(): inputs = jnp.concatenate(lax.all_gather(saved_input, 'tp'), axis=1)]
    all_gather x2, waiting for transfers between devices: 124 us -> 112 us  [in_one_piece(): out = lax.all_gather(both, axis, axis=dim, tiled=True)]
    reshape x0 -> x1, local copies, waits for them, and re-layouts: none -> 11.5 us  [body(): inputs = jnp.concatenate(lax.all_gather(saved_input, 'tp'), axis=1)]
  transfers between devices with their start and end apart: 4 -> 4, of which waited for: 4 -> 4; matrix products, arithmetic and copies ran while one was open for 1% -> 6% of each run, Pallas kernels for 0% -> 0%
where the time goes in v1:
time: 291 us; the launch traced here: 290 us
  waiting for transfers between devices  203 us (70%)
  blocking collectives  31.8 us (11%)
  local copies, waits for them, and re-layouts  20.8 us (7%)
  between operations  15.4 us (5%)
  matrix products  11.8 us (4%)
  starting transfers between devices  4.88 us (2%)
    all_gather x2, waiting for transfers between devices, in_one_piece(): out = lax.all_gather(both, axis, axis=dim, tiled=True)  112 us
    all_gather x1, waiting for transfers between devices, body(): inputs = jnp.concatenate(lax.all_gather(saved_input, 'tp'), axis=1)  83.7 us
    psum x2, blocking collectives, by_axis(): x = lax.psum(x, axis)  19 us
    all_to_all x1, blocking collectives, sent_and_summed(): pieces = lax.all_to_all(cut_along(x, dim, count), axis, 0, 0, tiled=True)  12.8 us
    reshape x1, local copies, waits for them, and re-layouts, body(): inputs = jnp.concatenate(lax.all_gather(saved_input, 'tp'), axis=1)  11.5 us
    dot_general x1, matrix products, body(): query_low = jnp.dot(inputs, bases[0], preferred_element_type=jnp.float32)  6.52 us
    all_to_all x1, waiting for transfers between devices, sent_to_all(): lax.all_to_all(jnp.broadcast_to(x[None], (count, *x.shape)), axis, 0, 0,...  6.45 us
    unnamed x32, local copies, waits for them, and re-layouts  6.26 us
  transfers between devices with their start and end apart: 4, of which 4 were waited for; matrix products, arithmetic and copies ran while one was open for 6% of the time, Pallas kernels for 0%

profile of v1, /device:TPU:2, one launch (start us, length us, event | category | flops | bytes accessed | tf_op | source)
XLA Modules:
  0.0 289.9 jit_solution(745959100085935350)
XLA Ops:
  7.2 0.7 all-gather.9.cloned.1.call-update
  8.0 1.7 pad_maximum_fusion
  9.7 83.7 %all-gather.9.cloned.1.call-done = bf16[32768,128]{1,0:T(8,128)(2,1)} async-done(((bf16[1024,128]{1,0:T(8,128)(2,1)}), bf16[32768,128]{1,0:T(8,128)(2,1)}) %all-gather.9.cloned.1.call-update) | async-done | bytes 8388624 | tf_op jit(solution)/shard_map/all_gather | solution.py:107
  93.4 11.5 %copy.38 = bf16[1024,32,128]{0,2,1:T(8,128)(2,1)} copy(bf16[1024,32,128]{2,0,1:T(8,128)(2,1)} %bitcast.30) | data formatting | bytes 16777216 | tf_op jit(solution)/shard_map/reshape | solution.py:107
  104.8 55.4 %all-gather.5.cloned.1.call-done = bf16[4096,512]{1,0:T(8,128)(2,1)} async-done(((bf16[256,512]{1,0:T(8,128)(2,1)}), bf16[4096,512]{1,0:T(8,128)(2,1)}) %all-gather.5.cloned.1.call-update) | async-done | bytes 4194320 | tf_op jit(solution)/shard_map/all_gather | solution.py:20
  160.3 6.5 %fusion.4 = f32[1024,256]{0,1:T(8,128)S(1)} fusion(bf16[1024,4096]{0,1:T(8,128)(2,1)} %bitcast.28, bf16[4096,512]{1,0:T(8,128)(2,1)} %all-gather.5.cloned.1.call-done), kind=kOutput, calls=%fused_computation.4 | convolution fusion | flops 2147483648 | bytes 11534336 | tf_op jit(solution)/shard_map/dot_general | solution.py:109
  166.8 0.3 fusion.14
  167.2 0.3 convolution_add_fusion.1
  167.5 0.4 copy-done.2
  167.9 2.3 fusion.7
  170.3 0.3 fusion.11
  170.7 0.3 convolution_add_fusion
  171.0 0.1 copy.39
  171.1 12.8 %all_to_all.10 = f32[16,16,256]{2,1,0:T(8,128)S(1)} all-to-all(f32[16,16,256]{2,1,0:T(8,128)S(1)} %bitcast.31), channel_id=1, replica_groups=mesh['fs_0'=4,'fs_1'=4,'tp'=32] {'fs_0','fs_1'}, dimensions={0} | all-to-all | bytes 524288 | tf_op jit(solution)/shard_map/all_to_all | solution.py:32
  184.1 0.7 broadcast_in_dim.2
  184.7 4.8 %all-to-all-start.1 = ((bf16[16,16,256]{2,1,0:T(8,128)(2,1)}), bf16[16,16,256]{2,1,0:T(8,128)(2,1)S(1)}, u32[]{:S(2)}, u32[]{:S(2)}) async-start(bf16[16,16,256]{2,1,0:T(8,128)(2,1)} %broadcast_in_dim.2), calls=%async_computation.1 | async-start | bytes 262144 | tf_op jit(solution)/shard_map/all_to_all | solution.py:38
  189.6 0.1 copy.40
  189.8 6.4 %all-to-all-done.1 = bf16[16,16,256]{2,1,0:T(8,128)(2,1)S(1)} async-done(((bf16[16,16,256]{2,1,0:T(8,128)(2,1)}), bf16[16,16,256]{2,1,0:T(8,128)(2,1)S(1)}, u32[]{:S(2)}, u32[]{:S(2)}) %all-to-all-start.1) | async-done | bytes 131104 | tf_op jit(solution)/shard_map/all_to_all | solution.py:38
  196.2 0.8 multiply_reduce_fusion
  197.0 0.8 multiply_reduce_fusion.1
  197.9 9.2 %all-reduce.1 = (f32[1]{0:T(128)}, f32[1]{0:T(128)}) all-reduce(f32[1]{0:T(128)} %bitcast.7, f32[1]{0:T(128)} %bitcast.10), channel_id=1, replica_groups=mesh['fs_0'=4,'fs_1'=4,'tp'=32] {'fs_0'}, use_global_device_ids=true, to_apply=%region_2.0 | all-reduce | flops 2 | bytes 16 | tf_op jit(solution)/shard_map/psum | solution.py:54
  207.0 9.8 %all-reduce = (f32[1]{0:T(128)}, f32[1]{0:T(128)}) all-reduce(f32[1]{0:T(128)} %get-tuple-element.42, f32[1]{0:T(128)} %get-tuple-element.43), channel_id=1, replica_groups=mesh['fs_0'=4,'fs_1'=4,'tp'=32] {'fs_1'}, use_global_device_ids=true, to_apply=%region_3.0 | all-reduce | flops 2 | bytes 16 | tf_op jit(solution)/shard_map/psum | solution.py:54
  218.3 0.7 pad_maximum_fusion.2
  219.0 0.6 fusion.27
  219.6 0.8 copy.43
  220.3 0.8 copy.42
  221.1 0.8 copy.46
  221.9 0.8 copy.45
  222.6 56.5 %all-gather.7.cloned.1.call-done = bf16[4096,256]{0,1:T(8,128)(2,1)} async-done(((bf16[256,256]{0,1:T(8,128)(2,1)}), bf16[4096,256]{0,1:T(8,128)(2,1)}) %all-gather.7.cloned.1.call-update) | async-done | bytes 2097168 | tf_op jit(solution)/shard_map/all_gather | solution.py:20
  279.1 1.7 fusion.26
  280.8 1.3 copy.47
  282.1 1.3 copy.44
  (33 shorter events, 0.4 us)
Async XLA Ops:
  7.2 159.6 %copy-start = (bf16[1024,128]{1,0:T(8,128)(2,1)S(1)}, bf16[1024,128]{1,0:T(8,128)(2,1)}, u32[]{:S(2)}) copy-start(bf16[1024,128]{1,0:T(8,128)(2,1)} %param.12) | copy-start | bytes 786436
  7.2 86.2 %all-gather.9.cloned.1.call-start = ((), (), s32[]{:S(2)}) async-start(), calls=%async_computation.4 | async-start | bytes 8650752 | tf_op jit(solution)/shard_map/all_gather | solution.py:107
  7.9 152.4 %all-gather.5.cloned.1.call-start = ((), (), s32[]{:S(2)}) async-start(), calls=%async_computation.2 | async-start | bytes 4456448 | tf_op jit(solution)/shard_map/all_gather | solution.py:20
  160.3 7.2 %copy-start.1 = (bf16[1024,32,128]{0,2,1:T(8,128)(2,1)S(1)}, bf16[1024,32,128]{0,2,1:T(8,128)(2,1)}, u32[]{:S(2)}) copy-start(bf16[1024,32,128]{0,2,1:T(8,128)(2,1)} %copy.38) | copy-start | bytes 25165828
  160.3 7.6 %copy-start.2 = (bf16[4096,512]{1,0:T(8,128)(2,1)S(1)}, bf16[4096,512]{1,0:T(8,128)(2,1)}, u32[]{:S(2)}) copy-start(bf16[4096,512]{1,0:T(8,128)(2,1)} %all-gather.5.cloned.1.call-done) | copy-start | bytes 12582916
  167.9 2.3 copy-start.3
  170.2 13.8 %copy-start.8 = (f32[16,128]{1,0:T(8,128)S(1)}, f32[16,128]{1,0:T(8,128)}, u32[]{:S(2)}) copy-start(f32[16,128]{1,0:T(8,128)} %param.21) | copy-start | bytes 24580
  170.2 13.8 %copy-start.9 = (f32[16,128]{1,0:T(8,128)S(1)}, f32[16,128]{1,0:T(8,128)}, u32[]{:S(2)}) copy-start(f32[16,128]{1,0:T(8,128)} %param.19) | copy-start | bytes 24580
  170.3 13.8 %copy-start.10 = (f32[16,128]{1,0:T(8,128)S(1)}, f32[16,128]{1,0:T(8,128)}, u32[]{:S(2)}) copy-start(f32[16,128]{1,0:T(8,128)} %param.20) | copy-start | bytes 24580
  170.3 13.8 %copy-start.11 = (f32[16,128]{1,0:T(8,128)S(1)}, f32[16,128]{1,0:T(8,128)}, u32[]{:S(2)}) copy-start(f32[16,128]{1,0:T(8,128)} %param.18) | copy-start | bytes 24580
  170.3 19.3 %copy-start.6 = (f32[256,128]{1,0:T(8,128)S(1)}, f32[256,128]{1,0:T(8,128)}, u32[]{:S(2)}) copy-start(f32[256,128]{1,0:T(8,128)} %param.14) | copy-start | bytes 393220
  170.3 19.4 %copy-start.7 = (f32[256,128]{1,0:T(8,128)S(1)}, f32[256,128]{1,0:T(8,128)}, u32[]{:S(2)}) copy-start(f32[256,128]{1,0:T(8,128)} %param.15) | copy-start | bytes 393220
  170.3 25.9 %copy-start.4 = (bf16[256,256]{1,0:T(8,128)(2,1)S(1)}, bf16[256,256]{1,0:T(8,128)(2,1)}, u32[]{:S(2)}) copy-start(bf16[256,256]{1,0:T(8,128)(2,1)} %param.17) | copy-start | bytes 393220
  170.3 26.7 %copy-start.5 = (bf16[256,256]{1,0:T(8,128)(2,1)S(1)}, bf16[256,256]{1,0:T(8,128)(2,1)}, u32[]{:S(2)}) copy-start(bf16[256,256]{1,0:T(8,128)(2,1)} %param.16) | copy-start | bytes 393220
  184.7 11.5 %all-to-all-start.1 = ((bf16[16,16,256]{2,1,0:T(8,128)(2,1)}), bf16[16,16,256]{2,1,0:T(8,128)(2,1)S(1)}, u32[]{:S(2)}, u32[]{:S(2)}) async-start(bf16[16,16,256]{2,1,0:T(8,128)(2,1)} %broadcast_in_dim.2), calls=%async_computation.1 | async-start | bytes 262144 | tf_op jit(solution)/shard_map/all_to_all | solution.py:38
  189.5 89.6 %all-gather.7.cloned.1.call-start = ((), (), s32[]{:S(2)}) async-start(), calls=%async_computation.3 | async-start | bytes 2228224 | tf_op jit(solution)/shard_map/all_gather | solution.py:20
Sparse Core Ops, SparseCore 0:
  10.1 83.2 all-gather.8
  97.0 63.2 all-gather.4
  219.1 59.9 all-gather.6
